TPU v7x, 128 devices: a whole 4x4x4 slice. The times are simulated.
128 devices in a mesh: sp: 32 (over z, y, core), tp: 4 (over x).
Axes of the slice: x: 4, y: 4, z: 4, core: 2. Of those that a mesh axis runs over, the one named last changes fastest.
Arguments:
- residual: bfloat16 [32768, 2048], P('sp'), may hold values from -6 to 6
- small_heads: bfloat16 [32768, 1024], P('sp', 'tp'), may hold values from -6 to 6
- large_heads: bfloat16 [32768, 1024], P('sp', 'tp'), may hold values from -6 to 6
- state_keys: bfloat16 [32768, 8, 128], P('sp', 'tp'), may hold values from -6 to 6
- state_queries: bfloat16 [32768, 8, 128], P('sp', 'tp'), may hold values from -6 to 6
- small_gate: bfloat16 [32768, 1024], P('sp', 'tp'), may hold values from -6 to 6
- large_gate: bfloat16 [32768, 1024], P('sp', 'tp'), may hold values from -6 to 6
- small_step: float32 [32768, 16], P('sp', 'tp'), may hold values from -3 to 2
- large_step: float32 [32768, 8], P('sp', 'tp'), may hold values from -3 to 2
- small_taps: bfloat16 [4, 1024], P(None, 'tp'), may hold values from -3 to 3
- large_taps: bfloat16 [4, 1024], P(None, 'tp'), may hold values from -3 to 3
- key_taps: bfloat16 [4, 8, 128], P(None, 'tp'), may hold values from -3 to 3
- query_taps: bfloat16 [4, 8, 128], P(None, 'tp'), may hold values from -3 to 3
- small_decay: float32 [16], P('tp'), may hold values from -12 to -2, as said below
- large_decay: float32 [8], P('tp'), may hold values from -12 to -2, as said below
- small_gain: bfloat16 [1024], P('tp'), may hold values from 0.099609375 to 1.8984375
- large_gain: bfloat16 [1024], P('tp'), may hold values from 0.099609375 to 1.8984375
- small_out: bfloat16 [1024, 2048], P('tp'), may hold values from -0.125 to 0.125
- large_out: bfloat16 [1024, 2048], P('tp'), may hold values from -0.125 to 0.125
- mixer_gain: bfloat16 [2048], replicated, may hold values from 0.099609375 to 1.8984375
- ffn_in_gain: bfloat16 [2048], replicated, may hold values from 0.099609375 to 1.8984375
- gate_proj: bfloat16 [2048, 5632], P('sp', 'tp'), may hold values from -0.125 to 0.125
- up_proj: bfloat16 [2048, 5632], P('sp', 'tp'), may hold values from -0.125 to 0.125
- down_proj: bfloat16 [2048, 5632], P('sp', 'tp'), may hold values from -0.078125 to 0.078125
- ffn_out_gain: bfloat16 [2048], replicated, may hold values from 0.099609375 to 1.8984375
Outputs:
- updated: bfloat16 [32768, 2048], P(('sp', 'tp'))
Inputs may be any that keep to these rules, and one draw needn't show every extreme that they name: `small_decay`: log decay rates of the first group. `large_decay`: log decay rates of the second group.
All inputs are finite; a program needn't handle non-finite values.
Results may differ from a plain program's by a relative error of at most 0.014.
Values may be sent and summed in bfloat16 or wider, within the bound.
No kernel may reach another device: no remote copies, remote signals or barrier semaphores. Data moves between devices by JAX's collectives and lax.ppermute only.
A program may use at most 192 MiB of HBM per device.

v0:
```python
import jax
import jax.numpy as jnp
from jax import lax
from jax.sharding import Mesh
from jax.sharding import PartitionSpec as P

BLOCK = 128
SP = ("sp_0", "sp_1", "sp_2")
SP_TP = ("sp_0", "sp_1", "sp_2", "tp")


EPS = 1e-06


def passed_along(block, axis, distance):
    devices = range(lax.axis_size(axis))
    route = [(i - distance, i) for i in devices if i - distance in devices]
    return lax.ppermute(block, axis, route)


def nothing_yet(array, identity):
    return jax.tree.map(
        lambda a, e: jnp.broadcast_to(jnp.asarray(e, a.dtype), a.shape), array, identity
    )


def collected_together(array, axis):
    leaves = jax.tree.leaves(array)
    sequence = sorted(range(len(leaves)), key=lambda k: -leaves[k].size)
    width = (1, *leaves[sequence[0]].shape)[-1]
    lines = [
        jnp.pad(leaves[k].reshape(-1), (0, -leaves[k].size % width)).reshape(-1, width)
        for k in sequence
    ]
    both, at, found = (lax.all_gather(jnp.concatenate(lines), axis), 0, {})
    for k, line in zip(sequence, lines):
        slab = both[:, at : at + len(line)].reshape(len(both), -1)
        found[k] = slab[:, : leaves[k].size].reshape(-1, *leaves[k].shape)
        at += len(line)
    numbers = iter(range(len(leaves)))
    return jax.tree.map(lambda _: found[next(numbers)], array)


def prefix_by_axis(array, axes, combine, identity):
    before = start = nothing_yet(array, identity)
    subtotal = array
    for axis in reversed(axes):
        peers, position = (lax.axis_size(axis), lax.axis_index(axis))
        pieces = collected_together(
            jax.tree.map(
                lambda part, kind: part.astype(kind),
                subtotal,
                (jnp.bfloat16, jnp.bfloat16, jnp.bfloat16, jnp.bfloat16),
            ),
            axis,
        )
        inside, subtotal = (start, start)
        for k in range(peers):
            passed = k < position
            subtotal = combine(
                subtotal, jax.tree.map(lambda part, own: part[k].astype(own.dtype), pieces, array)
            )
            inside = jax.tree.map(lambda new, old: jnp.where(passed, new, old), subtotal, inside)
        before = combine(inside, before)
    return before


def in_one_piece(arrays, axis, dim, along):
    both = jnp.concatenate(arrays, axis=along)
    whole, at, finished = (lax.all_gather(both, axis, axis=dim, tiled=True), 0, [])
    for a in arrays:
        finished.append(lax.slice_in_dim(whole, at, at + a.shape[along], axis=along))
        at += a.shape[along]
    return tuple(finished)


def in_order(pieces, dim):
    pieces = jnp.moveaxis(pieces, 0, dim)
    dims = pieces.shape
    return pieces.reshape(*dims[:dim], dims[dim] * dims[dim + 1], *dims[dim + 2 :])


def all_blocks(array, axes, sequence):
    pieces = array
    for k in sequence:
        pieces = lax.all_gather(pieces, axes[k])
    done = sequence[::-1]
    back = [done.index(k) for k in range(len(axes))]
    pieces = pieces.transpose(*back, *range(len(axes), pieces.ndim))
    return pieces.reshape(-1, *array.shape)


def gather_axes(array, axes, sequence, dim):
    return in_order(all_blocks(array, axes, sequence), dim)


def causal_taps(extended, tap_weights, length):
    kernel_len = tap_weights.shape[0]
    summed = jnp.zeros((length,) + extended.shape[1:], jnp.float32)
    for offset in range(kernel_len):
        window_rows = extended[offset : offset + length].astype(jnp.float32)
        summed = summed + tap_weights[offset].astype(jnp.float32) * window_rows
    return jax.nn.silu(summed).astype(jnp.bfloat16)


def block_pass(values, key_rows, queries, step_sizes, decay_rates):
    length, groups, head_count, head_dim = values.shape
    block_count = length // BLOCK
    state_len = key_rows.shape[-1]
    log_decay = -step_sizes * decay_rates
    causal = jnp.tril(jnp.ones((BLOCK, BLOCK), dtype=bool))

    def one_block(carry_state, block):
        block_values, block_keys, block_queries, block_steps, block_decay = block
        cumulative = jnp.cumsum(block_decay, axis=0)
        scores = jnp.einsum(
            "lgn,sgn->gls", block_queries, block_keys, preferred_element_type=jnp.float32
        )
        cum_heads = jnp.transpose(cumulative, (1, 2, 0))
        gap_matrix = cum_heads[:, :, :, None] - cum_heads[:, :, None, :]
        decays = jnp.exp(jnp.where(causal, gap_matrix, -jnp.inf))
        step_heads = jnp.transpose(block_steps, (1, 2, 0))[:, :, None, :]
        weights = (scores[:, None] * decays * step_heads).astype(jnp.bfloat16)
        inside = jnp.einsum(
            "ghls,sghp->lghp", weights, block_values, preferred_element_type=jnp.float32
        )
        carried = jnp.einsum("lgn,ghpn->lghp", block_queries.astype(jnp.float32), carry_state)
        carried = carried * jnp.exp(cumulative)[..., None]
        tail_sum = cumulative[-1]
        scaled = (
            block_values.astype(jnp.float32)
            * (block_steps * jnp.exp(tail_sum - cumulative))[..., None]
        )
        fresh_state = jnp.einsum(
            "lghp,lgn->ghpn",
            scaled.astype(jnp.bfloat16),
            block_keys,
            preferred_element_type=jnp.float32,
        )
        next_state = carry_state * jnp.exp(tail_sum)[..., None, None] + fresh_state
        return (next_state, (inside + carried, cumulative))

    blocked = (
        values.reshape(block_count, BLOCK, groups, head_count, head_dim),
        key_rows.reshape(block_count, BLOCK, groups, state_len),
        queries.reshape(block_count, BLOCK, groups, state_len),
        step_sizes.reshape(block_count, BLOCK, groups, head_count),
        log_decay.reshape(block_count, BLOCK, groups, head_count),
    )
    start_state = jnp.zeros((groups, head_count, head_dim, state_len), jnp.float32)
    end_state, (outputs, cumulative) = lax.scan(one_block, start_state, blocked)
    tail_sums = cumulative[:, -1]
    offsets = jnp.cumsum(tail_sums, axis=0) - tail_sums
    device_cum = (cumulative + offsets[:, None]).reshape(length, groups, head_count)
    return (
        outputs.reshape(length, groups, head_count, head_dim),
        device_cum,
        end_state,
        jnp.sum(tail_sums, axis=0),
    )


def head_group(values, key_rows, queries, step_raw, decay_log):
    length = values.shape[0]
    head_count = step_raw.shape[1]
    groups = key_rows.shape[1]
    per_group = head_count // groups
    head_dim = values.shape[1] // head_count
    step_sizes = jax.nn.softplus(step_raw).reshape(length, groups, per_group)
    decay_rates = jnp.exp(decay_log).reshape(groups, per_group)
    return block_pass(
        values.reshape(length, groups, per_group, head_dim),
        key_rows,
        queries,
        step_sizes,
        decay_rates,
    )


def add_entering(outputs, queries, device_cum, entering):
    extra = jnp.einsum("lgn,ghpn->lghp", queries.astype(jnp.float32), entering)
    return outputs + extra * jnp.exp(device_cum)[..., None]


def unit_rms(values):
    return values * lax.rsqrt(jnp.mean(values * values, axis=-1, keepdims=True) + EPS)


def gate_and_norm(mixed_heads, gate_raw, gain):
    length, groups, per_group, head_dim = mixed_heads.shape
    gated = mixed_heads.reshape(length, -1) * jax.nn.silu(gate_raw.astype(jnp.float32))
    normed = unit_rms(gated.reshape(length, groups * per_group, head_dim))
    return (normed.reshape(length, -1) * gain.astype(jnp.float32)).astype(jnp.bfloat16)


def local(
    residual,
    small_heads,
    large_heads,
    state_keys,
    state_queries,
    small_gate,
    large_gate,
    small_step,
    large_step,
    small_taps,
    large_taps,
    key_taps,
    query_taps,
    small_decay,
    large_decay,
    small_gain,
    large_gain,
    small_out,
    large_out,
    mixer_gain,
    ffn_in_gain,
    gate_proj,
    up_proj,
    down_proj,
    ffn_out_gain,
):
    length = residual.shape[0]
    halo_rows = small_taps.shape[0] - 1
    first_row = length - halo_rows
    previous = passed_along(
        (
            small_heads[first_row:],
            large_heads[first_row:],
            state_keys[first_row:],
            state_queries[first_row:],
        ),
        SP,
        1,
    )
    small_conv = causal_taps(
        jnp.concatenate([previous[0], small_heads], axis=0), small_taps, length
    )
    large_conv = causal_taps(
        jnp.concatenate([previous[1], large_heads], axis=0), large_taps, length
    )
    key_conv = causal_taps(jnp.concatenate([previous[2], state_keys], axis=0), key_taps, length)
    query_conv = causal_taps(
        jnp.concatenate([previous[3], state_queries], axis=0), query_taps, length
    )
    small_out_local, small_cum, small_end, small_total = head_group(
        small_conv, key_conv[:, 0:1], query_conv[:, 0:1], small_step, small_decay
    )
    large_out_local, large_cum, large_end, large_total = head_group(
        large_conv, key_conv[:, 1:2], query_conv[:, 1:2], large_step, large_decay
    )

    def join(earlier, later):
        return (
            earlier[0] * jnp.exp(later[1])[..., None, None] + later[0],
            earlier[1] + later[1],
            earlier[2] * jnp.exp(later[3])[..., None, None] + later[2],
            earlier[3] + later[3],
        )

    identity_parts = (
        jnp.zeros_like(small_end),
        jnp.zeros_like(small_total),
        jnp.zeros_like(large_end),
        jnp.zeros_like(large_total),
    )
    entered = prefix_by_axis(
        (small_end, small_total, large_end, large_total), SP, join, identity_parts
    )
    small_enter = entered[0]
    large_enter = entered[2]
    small_mix = add_entering(small_out_local, query_conv[:, 0:1], small_cum, small_enter)
    large_mix = add_entering(large_out_local, query_conv[:, 1:2], large_cum, large_enter)
    small_normed = gate_and_norm(small_mix, small_gate, small_gain)
    large_normed = gate_and_norm(large_mix, large_gate, large_gain)
    partial_value = jnp.dot(small_normed, small_out, preferred_element_type=jnp.float32)
    partial_value = partial_value + jnp.dot(
        large_normed, large_out, preferred_element_type=jnp.float32
    )
    mix = lax.psum(partial_value.astype(jnp.bfloat16), "tp").astype(jnp.float32)
    mixed = residual.astype(jnp.float32) + unit_rms(mix) * mixer_gain.astype(jnp.float32)
    normed_in = (unit_rms(mixed) * ffn_in_gain.astype(jnp.float32)).astype(jnp.bfloat16)
    pieces = in_one_piece((gate_proj, up_proj), SP, 0, 1)
    gate = jnp.dot(normed_in, pieces[0], preferred_element_type=jnp.float32)
    up_values = jnp.dot(normed_in, pieces[1], preferred_element_type=jnp.float32)
    down_full = gather_axes(down_proj, (("sp_0", "sp_1"), "sp_2"), (0, 1), 0)
    hidden = (jax.nn.silu(gate) * up_values).astype(jnp.bfloat16)
    share = length // lax.axis_size("tp")
    ffn = lax.psum_scatter(
        lax.dot_general(
            hidden, down_full, (((1,), (1,)), ((), ())), preferred_element_type=jnp.float32
        ).astype(jnp.bfloat16),
        "tp",
        scatter_dimension=0,
        tiled=True,
    ).astype(jnp.float32)
    own_rows = lax.dynamic_slice_in_dim(mixed, lax.axis_index("tp") * share, share, 0)
    updated = own_rows + 0.5 * unit_rms(ffn) * ffn_out_gain.astype(jnp.float32)
    return updated.astype(jnp.bfloat16)


def solution(mesh):
    torus = Mesh(mesh.devices.reshape(4, 4, 2, mesh.shape["tp"]), ("sp_0", "sp_1", "sp_2", "tp"))
    in_specs = (
        P(SP, None),
        P(SP, "tp"),
        P(SP, "tp"),
        P(SP, "tp", None),
        P(SP, "tp", None),
        P(SP, "tp"),
        P(SP, "tp"),
        P(SP, "tp"),
        P(SP, "tp"),
        P(None, "tp"),
        P(None, "tp"),
        P(None, "tp", None),
        P(None, "tp", None),
        P("tp"),
        P("tp"),
        P("tp"),
        P("tp"),
        P("tp", None),
        P("tp", None),
        P(),
        P(),
        P(SP, "tp"),
        P(SP, "tp"),
        P(SP, "tp"),
        P(),
    )
    out_specs = P(SP_TP, None)
    return jax.shard_map(local, mesh=torus, in_specs=in_specs, out_specs=out_specs, check_vma=False)
```

profile of v0, /device:TPU:1, one launch (start us, length us, event | category | flops | bytes accessed | tf_op | source)
XLA Modules:
  0.0 482.5 jit_solution(811788357132697715)
XLA Ops:
  9.0 4.6 collective-permute-start
  49.2 83.8 %while.30 = (s32[]{:T(128)}, f32[1,4,64,128]{3,2,1,0:T(8,128)S(1)}, f32[8,128,1,4,64]{1,0,4,3,2:T(8,128)}, f32[8,128,1,4]{3,1,2,0:T(8,128)}, f32[8,128,1,4]{3,1,...) while((s32[]{:T(128)}, f32[1,4,64,128]{3,2,1,0:T(8,128)S(1)}, ...), condition=%wide.region_2.3_spmd.clone, body=%wide.region_0.2_spmd.clone.sunk | while | flops 30065156 | bytes 1596155 | solution.py:151
  54.6 4.4 dynamic_update_slice.27
  65.1 4.4 dynamic_update_slice.27
  75.6 4.4 dynamic_update_slice.27
  86.0 4.4 dynamic_update_slice.27
  96.5 4.4 dynamic_update_slice.27
  138.7 86.1 %while.31 = (s32[]{:T(128)}, f32[1,2,128,128]{3,2,1,0:T(8,128)S(1)}, f32[8,128,1,2,128]{1,0,4,3,2:T(8,128)}, f32[8,128,1,2]{3,1,2,0:T(8,128)}, f32[8,128,1,2]{3,...) while((s32[]{:T(128)}, ...), condition=%wide.region_5.6_spmd.clone, body=%wide.region_3.5_spmd.clone.sunk | while | flops 29868292 | bytes 1569483 | solution.py:151
  144.1 4.8 dynamic_update_slice.29
  154.9 4.8 dynamic_update_slice.29
  165.7 4.8 dynamic_update_slice.29
  176.4 4.8 dynamic_update_slice.29
  187.2 4.8 dynamic_update_slice.29
  198.0 4.8 dynamic_update_slice.29
  208.7 4.8 dynamic_update_slice.29
  219.5 4.8 dynamic_update_slice.29
  228.6 11.5 %all-gather.6 = bf16[4,514,128]{2,1,0:T(8,128)(2,1)S(1)} all-gather(bf16[1,514,128]{2,1,0:T(8,128)(2,1)S(1)} %maximum_bitcast_fusion.1), channel_id=3, replica_groups=mesh['sp_0'=4,'sp_1'=4,'sp_2'=2,'tp'=4] {'sp_1'}, dimensions={0}, use_global_device_ids=true | all-gather | bytes 657920 | tf_op jit(solution)/shard_map/all_gather | solution.py:35
  241.5 10.9 %all-gather.7 = bf16[4,514,128]{2,1,0:T(8,128)(2,1)S(1)} all-gather(bf16[1,514,128]{2,1,0:T(8,128)(2,1)S(1)} %maximum_bitcast_fusion.2), channel_id=4, replica_groups=mesh['sp_0'=4,'sp_1'=4,'sp_2'=2,'tp'=4] {'sp_0'}, dimensions={0}, use_global_device_ids=true | all-gather | bytes 657920 | tf_op jit(solution)/shard_map/all_gather | solution.py:35
  279.7 94.6 %all-reduce.8.cloned.1.call-done = bf16[1024,2048]{1,0:T(8,128)(2,1)} async-done(((bf16[1024,2048]{1,0:T(8,128)(2,1)}), bf16[1024,2048]{1,0:T(8,128)(2,1)}) %all-reduce.8.cloned.1.call-update) | async-done | bytes 4194320 | tf_op jit(solution)/shard_map/psum | solution.py:280
  377.8 6.0 %multiply_reduce_fusion = (f32[1024]{0:T(1024)S(1)}, f32[1024,2048]{1,0:T(8,128)}) fusion(f32[2048]{0:T(1024)S(1)} %convert_element_type.718, f32[1024]{0:T(1024)S(1)} %add_rsqrt_fusion.3, bf16[1024,2048]{1,0:T(8,128)(2,1)S(1)} %copy-done.2, bf16[1024,2048]{1,0:T(8,128)(2,1)} %param.29), kind=kLoop, calls=%fused_computation.98 | loop fusion | flops 14679040 | bytes 16793600 | tf_op jit(solution)/shard_map/reduce_sum | solution.py:186
  383.8 5.8 %copy.254 = bf16[16,2,64,1408]{3,2,1,0:T(8,128)(2,1)} copy(bf16[16,2,64,1408]{3,2,0,1:T(8,128)(2,1)} %bitcast.557) | data formatting | bytes 11534336 | tf_op jit(solution)/shard_map/transpose | solution.py:89
  389.6 12.6 %fusion.79 = f32[1024,1408]{1,0:T(8,128)} fusion(bf16[2048,2816]{1,0:T(8,128)(2,1)} %all-gather.12.cloned.1.call-done, f32[1024,2048]{1,0:T(8,128)} %get-tuple-element.310, f32[2048]{0:T(1024)S(1)} %convert_element_type.719, f32[1024]{0:T(1024)S(1)} %add_rsqrt_fusion.2), kind=kOutput, calls=%fused_computation.102 | convolution fusion | flops 5911871488 | bytes 19935232 | tf_op jit(solution)/shard_map/dot_general | solution.py:284
  402.2 21.5 %fusion.86 = bf16[1024,2048]{1,0:T(8,128)(2,1)} fusion(bf16[2048,1408]{1,0:T(8,128)(2,1)} %bitcast.558, f32[1024,1408]{1,0:T(8,128)} %fusion.79, bf16[2048,2816]{1,0:T(8,128)(2,1)} %all-gather.12.cloned.1.call-done, f32[1024,2048]{1,0:T(8,128)} %get-tuple-element.310, f32[2048]{0:T(1024)S(1)} %convert_element_type.719, f32[1024]{0:T(1024)S(1)} %add_rsqrt_fusion.2), kind=kOutput, calls=%fused_computation.106 | convolution fusion | flops 11828199424 | bytes 29896704 | tf_op jit(solution)/shard_map/dot_general | solution.py:290
  423.7 46.8 %reduce-scatter.2.cloned.1.call-done = bf16[256,2048]{1,0:T(8,128)(2,1)} async-done(((bf16[1024,2048]{1,0:T(8,128)(2,1)}), bf16[256,2048]{1,0:T(8,128)(2,1)}) %reduce-scatter.2.cloned.1.call-update) | async-done | bytes 1048592 | tf_op jit(solution)/shard_map/reduce_scatter | solution.py:289
  (461 shorter events, 192.1 us)
Async XLA Ops:
  7.4 265.7 %copy-start = (bf16[256,2048]{1,0:T(8,128)(2,1)S(1)}, bf16[256,2048]{1,0:T(8,128)(2,1)}, u32[]{:S(2)}) copy-start(bf16[256,2048]{1,0:T(8,128)(2,1)} %param.46) | copy-start | bytes 3145732
  7.4 31.6 %copy-start.12 = (bf16[256]{0:T(256)(128)(2,1)S(1)}, bf16[256]{0:T(256)(128)(2,1)}, u32[]{:S(2)}) copy-start(bf16[256]{0:T(256)(128)(2,1)} %param.45) | copy-start | bytes 1540
  7.4 270.4 %all-gather.14.cloned.1.call-start = ((), (), s32[]{:S(2)}) async-start(), calls=%async_computation.4 | async-start | bytes 3063808 | tf_op jit(solution)/shard_map/all_gather | solution.py:86
  8.1 366.2 %all-reduce.8.cloned.1.call-start = ((), (), s32[]{:S(2)}) async-start(), calls=%async_computation.1 | async-start | bytes 8388608 | tf_op jit(solution)/shard_map/psum | solution.py:280
  9.0 32.0 %collective-permute-start = (bf16[3,256]{0,1:T(8,128)(2,1)S(1)}, bf16[3,256]{0,1:T(8,128)(2,1)S(1)}, u32[]{:S(2)}, u32[]{:S(2)}) collective-permute-start(bf16[3,256]{0,1:T(8,128)(2,1)S(1)} %copy.225), channel_id=1, source_target_pairs={{0,4},{4,8},{8,12},{12,16},{16,20},{20,24},{24,28},{28,32},{32,36}... | collective-permute-start | bytes 4616 | tf_op jit(solution)/shard_map/ppermute | solution.py:18
  14.7 25.6 %collective-permute-start.1 = (bf16[3,2,128]{2,0,1:T(4,128)(2,1)S(1)}, bf16[3,2,128]{2,0,1:T(4,128)(2,1)S(1)}, u32[]{:S(2)}, u32[]{:S(2)}) collective-permute-start(bf16[3,2,128]{2,0,1:T(4,128)(2,1)S(1)} %slice.452), channel_id=1, source_target_pairs={{0,4},{4,8},{8,12},{12,16},{16,20},{20,24},{24,28},{28,32},{32,36}... | collective-permute-start | bytes 4616 | tf_op jit(solution)/shard_map/ppermute | solution.py:18
  17.7 0.8 copy-start.5
  18.5 27.4 %collective-permute-start.2 = (bf16[3,2,128]{2,0,1:T(4,128)(2,1)S(1)}, bf16[3,2,128]{2,0,1:T(4,128)(2,1)S(1)}, u32[]{:S(2)}, u32[]{:S(2)}) collective-permute-start(bf16[3,2,128]{2,0,1:T(4,128)(2,1)S(1)} %slice.458), channel_id=1, source_target_pairs={{0,4},{4,8},{8,12},{12,16},{16,20},{20,24},{24,28},{28,32},{32,36}... | collective-permute-start | bytes 4616 | tf_op jit(solution)/shard_map/ppermute | solution.py:18
  23.0 111.7 %collective-permute-start.3 = (bf16[3,256]{0,1:T(8,128)(2,1)S(1)}, bf16[3,256]{0,1:T(8,128)(2,1)S(1)}, u32[]{:S(2)}, u32[]{:S(2)}) collective-permute-start(bf16[3,256]{0,1:T(8,128)(2,1)S(1)} %copy.239), channel_id=1, source_target_pairs={{0,4},{4,8},{8,12},{12,16},{16,20},{20,24},{24,28},{28,32},{32,36}... | collective-permute-start | bytes 4616 | tf_op jit(solution)/shard_map/ppermute | solution.py:18
  252.5 0.8 copy-start.4
  266.2 5.7 %copy-start.3 = (f32[1024,1,2,128]{0,3,2,1:T(8,128)S(1)}, f32[1024,1,2,128]{0,3,2,1:T(8,128)}, u32[]{:S(2)}) copy-start(f32[1024,1,2,128]{0,3,2,1:T(8,128)} %reshape.977) | copy-start | bytes 3145732
  272.7 1.7 copy-start.6
  277.6 0.9 copy-start.7
  277.6 1.0 copy-start.8
  277.6 2.1 copy-start.9
  277.6 2.1 copy-start.10
  277.7 106.1 %all-gather.16.cloned.1.call-start = ((), (), s32[]{:S(2)}) async-start(), calls=%async_computation.5 | async-start | bytes 8650752 | tf_op jit(solution)/shard_map/all_gather | solution.py:86
  278.4 111.1 %all-gather.12.cloned.1.call-start = ((), (), s32[]{:S(2)}) async-start(), calls=%async_computation.2 | async-start | bytes 11894784 | tf_op jit(solution)/shard_map/all_gather | solution.py:70
  279.4 191.1 %reduce-scatter.2.cloned.1.call-start = ((), (), s32[]{:S(2)}) async-start(), calls=%async_computation.3 | async-start | bytes 5242880 | tf_op jit(solution)/shard_map/reduce_scatter | solution.py:289
  374.3 3.4 copy-start.2
  402.2 21.6 %copy-start.11 = (bf16[2048]{0:T(1024)(128)(2,1)S(1)}, bf16[2048]{0:T(1024)(128)(2,1)}, u32[]{:S(2)}) copy-start(bf16[2048]{0:T(1024)(128)(2,1)} %param.53) | copy-start | bytes 12292
  402.2 73.2 %copy-start.1 = (bf16[256,2048]{1,0:T(8,128)(2,1)S(1)}, bf16[256,2048]{1,0:T(8,128)(2,1)}, u32[]{:S(2)}) copy-start(bf16[256,2048]{1,0:T(8,128)(2,1)} %param.46) | copy-start | bytes 3145732
Sparse Core Ops, SparseCore 0:
  10.3 49.5 all-gather.13
  280.1 23.3 all-gather.15
  305.8 61.5 all-gather.11
Sparse Core Ops, SparseCore 1:
  277.7 96.5 all-reduce.7
  423.8 46.7 reduce-scatter.1
where the time goes:
time: 490 us; the launch traced here: 482 us
  waiting for transfers between devices  143 us (29%)
  local copies, waits for them, and re-layouts  137 us (28%)
  matrix products  104 us (21%)
  other arithmetic  45 us (9%)
  blocking collectives  24.6 us (5%)
  between operations  15.1 us (3%)
  starting transfers between devices  12.4 us (3%)
    psum x1, waiting for transfers between devices, local(): mix = lax.psum(partial_value.astype(jnp.bfloat16), 'tp').astype(jnp.float32)  94.6 us
    dynamic_update_slice x32, local copies, waits for them, and re-layouts, block_pass(): end_state, (outputs, cumulative) = lax.scan(one_block, start_state, blocked)  83.5 us
    reduce_scatter x1, waiting for transfers between devices, local(): lax.psum_scatter(lax.dot_general(hidden, down_full, (((1,), (1,)), ((), (...  46.8 us
    all_gather x3, blocking collectives, collected_together(): both, at, found = (lax.all_gather(jnp.concatenate(lines), axis), 0, {})  24.6 us
    dot_general x1, matrix products, local(): lax.dot_general(hidden, down_full, (((1,), (1,)), ((), ())), preferred_el...  21.5 us
    dot_general x16, matrix products, one_block(): jnp.einsum('ghls,sghp->lghp', weights, block_values, preferred_element_ty...  17.7 us
    dot_general x16, matrix products, one_block(): jnp.einsum('lghp,lgn->ghpn', scaled.astype(jnp.bfloat16), block_keys, pre...  16.3 us
    dynamic_slice x48, local copies, waits for them, and re-layouts, block_pass(): end_state, (outputs, cumulative) = lax.scan(one_block, start_state, blocked)  15.4 us
  transfers between devices with their start and end apart: 9, of which 2 were waited for; matrix products, arithmetic and copies ran while one was open for 51% of the time, Pallas kernels for 0%

commit v1 on v0

v1 whole, which is shorter than its diff:
```python
import jax
import jax.numpy as jnp
from jax import lax
from jax.experimental import pallas as pl
from jax.experimental.pallas import tpu as pltpu
from jax.sharding import Mesh
from jax.sharding import PartitionSpec as P

BLOCK = 128
HALO = 16
EPS = 1e-06
F32 = jnp.float32
BF16 = jnp.bfloat16


def cost(us):
    return pl.CostEstimate(flops=int(us * 2.5e8), bytes_accessed=int(us * 1e5), transcendentals=0)


def column_pairs(wide):
    lane = lax.broadcasted_iota(jnp.int32, wide[0].shape, 1)
    low = lane < 64
    return jnp.concatenate(
        [jnp.where(low, wide[0], wide[1]), jnp.where(low, wide[2], wide[3]), wide[4], wide[5]],
        axis=1,
    )


def pack_body(small, large, keys, queries, out, wide):
    out[:, 0:256] = small[...]
    out[:, 256:512] = large[...]
    for n, ref in enumerate((keys, queries)):
        wide[...] = ref[...].astype(F32)
        for g in range(2):
            at = 512 + 256 * n + 128 * g
            out[:, at : at + 128] = wide[pl.ds(g, HALO, stride=2), :].astype(BF16)


def pack_halo(small, large, keys, queries):
    last = small.shape[0] // HALO - 1
    return pl.pallas_call(
        pack_body,
        grid=(1,),
        in_specs=[
            pl.BlockSpec((HALO, 256), lambda i: (last, 0)),
            pl.BlockSpec((HALO, 256), lambda i: (last, 0)),
            pl.BlockSpec((2 * HALO, 128), lambda i: (last, 0)),
            pl.BlockSpec((2 * HALO, 128), lambda i: (last, 0)),
        ],
        out_specs=pl.BlockSpec((HALO, 1024), lambda i: (0, 0)),
        out_shape=jax.ShapeDtypeStruct((HALO, 1024), BF16),
        scratch_shapes=[pltpu.VMEM((2 * HALO, 128), F32)],
        name="pack_halo",
        cost_estimate=cost(1),
    )(small, large, keys, queries)


def put_state(ref, state, total):
    ref[0:BLOCK, :] = state.astype(BF16)
    high = total.astype(BF16)
    low = (total - high.astype(F32)).astype(BF16)
    ref[BLOCK : BLOCK + 16, :] = jnp.concatenate([high, low], axis=0)


def get_state(piece):
    piece = piece.astype(F32)
    return piece[0:BLOCK, :], piece[BLOCK : BLOCK + 8, :] + piece[BLOCK + 8 : BLOCK + 16, :]


def then(earlier, later):
    return earlier[0] * jnp.exp(later[1][0:1, :]) + later[0], earlier[1] + later[1]


def mixer_body(
    core,
    small_decay,
    large_decay,
    halo,
    small,
    large,
    keys,
    queries,
    small_step,
    large_step,
    small_taps,
    large_taps,
    key_taps,
    query_taps,
    mix_out,
    query_out,
    cum_out,
    keep_out,
    send_out,
    ext,
    wide,
    rows,
    state,
    total_rows,
    total_cols,
):
    step = pl.program_id(0)

    @pl.when(step == 0)
    def _():
        ext[0:8, :] = halo[...].astype(F32)[HALO - 8 :, :]
        state[...] = jnp.zeros_like(state)
        total_rows[...] = jnp.zeros_like(total_rows)
        total_cols[...] = jnp.zeros_like(total_cols)

    @pl.when(step > 0)
    def _():
        ext[0:8, :] = ext[BLOCK : BLOCK + 8, :]

    ext[8:, 0:256] = small[...].astype(F32)
    ext[8:, 256:512] = large[...].astype(F32)
    for n, ref in enumerate((keys, queries)):
        wide[n] = ref[...].astype(F32)
        for g in range(2):
            at = 512 + 256 * n + 128 * g
            ext[8:, at : at + 128] = wide[n, pl.ds(g, BLOCK, stride=2), :]

    kt = key_taps[...].astype(F32)
    qt = query_taps[...].astype(F32)
    st = small_taps[...].astype(F32)
    lt = large_taps[...].astype(F32)

    def conv(at, tap_rows):
        summed = tap_rows[0] * ext[5 : 5 + BLOCK, at : at + 128]
        for k in range(1, 4):
            summed = summed + tap_rows[k] * ext[5 + k : 5 + k + BLOCK, at : at + 128]
        return (summed * jax.nn.sigmoid(summed)).astype(BF16)

    values = [conv(128 * n, [st[k : k + 1, 128 * n : 128 * n + 128] for k in range(4)]) for n in range(2)]
    values += [
        conv(256 + 128 * n, [lt[k : k + 1, 128 * n : 128 * n + 128] for k in range(4)]) for n in range(2)
    ]
    key = [conv(512 + 128 * g, [kt[2 * k + g : 2 * k + g + 1, :] for k in range(4)]) for g in range(2)]
    query = [conv(768 + 128 * g, [qt[2 * k + g : 2 * k + g + 1, :] for k in range(4)]) for g in range(2)]
    query_out[...] = jnp.concatenate(query, axis=1)

    rows[0, 0:4, :] = small_step[...]
    rows[0, 4:6, :] = large_step[...]
    rows[0, 6:8, :] = jnp.zeros((2, BLOCK), F32)
    raw = rows[0]
    dt = jnp.maximum(raw, 0.0) + jnp.log1p(jnp.exp(-jnp.abs(raw)))
    for h in range(8):
        if h < 6:
            log_rate = small_decay[h] if h < 4 else large_decay[h - 4]
            rows[1, h : h + 1, :] = jnp.exp(jnp.full((1, BLOCK), log_rate, F32))
        else:
            rows[1, h : h + 1, :] = jnp.zeros((1, BLOCK), F32)
    decay = -dt * rows[1]
    r = lax.broadcasted_iota(jnp.int32, (BLOCK, BLOCK), 0)
    c = lax.broadcasted_iota(jnp.int32, (BLOCK, BLOCK), 1)
    upper = (r <= c).astype(F32)
    causal = c <= r
    cum = jnp.dot(decay, upper, precision=lax.Precision.HIGHEST, preferred_element_type=F32)
    tail = jnp.broadcast_to(cum[:, BLOCK - 1 : BLOCK], cum.shape)
    cum_out[...] = cum + total_rows[...]
    total_rows[...] = total_rows[...] + tail
    factor = dt * jnp.exp(tail - cum)
    cum_t = cum.T
    factor_t = factor.T
    cum_b = [jnp.broadcast_to(cum_t[:, h : h + 1], (BLOCK, BLOCK)) for h in range(6)]
    factor_b = [jnp.broadcast_to(factor_t[:, h : h + 1], (BLOCK, BLOCK)) for h in range(6)]
    cum_cols = column_pairs(cum_b)
    factor_cols = column_pairs(factor_b)
    tail_cols = cum_cols[BLOCK - 1 : BLOCK, :]

    scores = [
        lax.dot_general(query[g], key[g], (((1,), (1,)), ((), ())), preferred_element_type=F32)
        for g in range(2)
    ]
    inside = []
    for h in range(6):
        gap = cum_b[h] - cum[h : h + 1, :]
        decays = jnp.exp(jnp.where(causal, gap, -jnp.inf))
        weights = (scores[h // 4] * decays * dt[h : h + 1, :]).astype(BF16)
        if h < 4:
            inside.append(
                jnp.dot(weights, values[h // 2], preferred_element_type=F32)
            )
        else:
            inside.append(jnp.dot(weights, values[h - 2], preferred_element_type=F32))
    inside = column_pairs(inside)
    before = state[...].astype(BF16)
    carried = jnp.concatenate(
        [jnp.dot(query[g], before[:, 256 * g : 256 * g + 256], preferred_element_type=F32) for g in range(2)],
        axis=1,
    )
    mix_out[...] = inside + carried * jnp.exp(cum_cols)
    scaled = (jnp.concatenate(values, axis=1).astype(F32) * factor_cols).astype(BF16)
    fresh = jnp.concatenate(
        [
            lax.dot_general(
                key[g], scaled[:, 256 * g : 256 * g + 256], (((0,), (0,)), ((), ())), preferred_element_type=F32
            )
            for g in range(2)
        ],
        axis=1,
    )
    state[...] = state[...] * jnp.exp(tail_cols) + fresh
    total_cols[...] = total_cols[...] + tail_cols

    @pl.when(step == pl.num_programs(0) - 1)
    def _():
        first = core[0] == 0
        for ref, own in ((keep_out, first), (send_out, jnp.logical_not(first))):
            put_state(
                ref,
                jnp.where(own, state[:, 0:256], state[:, 256:512]),
                jnp.where(own, total_cols[:, 0:256], total_cols[:, 256:512]),
            )


def mixer(core, halo, small, large, keys, queries, small_step, large_step, small_taps, large_taps, key_taps, query_taps, small_decay, large_decay):
    length = small.shape[0]
    blocks = length // BLOCK
    whole = lambda *shape: pl.BlockSpec(shape, lambda i: (0,) * len(shape))
    return pl.pallas_call(
        mixer_body,
        grid=(blocks,),
        in_specs=[
            pl.BlockSpec(memory_space=pltpu.SMEM),
            pl.BlockSpec(memory_space=pltpu.SMEM),
            pl.BlockSpec(memory_space=pltpu.SMEM),
            whole(HALO, 1024),
            pl.BlockSpec((BLOCK, 256), lambda i: (i, 0)),
            pl.BlockSpec((BLOCK, 256), lambda i: (i, 0)),
            pl.BlockSpec((2 * BLOCK, 128), lambda i: (i, 0)),
            pl.BlockSpec((2 * BLOCK, 128), lambda i: (i, 0)),
            pl.BlockSpec((4, BLOCK), lambda i: (0, i)),
            pl.BlockSpec((2, BLOCK), lambda i: (0, i)),
            whole(4, 256),
            whole(4, 256),
            whole(8, 128),
            whole(8, 128),
        ],
        out_specs=[
            pl.BlockSpec((BLOCK, 512), lambda i: (i, 0)),
            pl.BlockSpec((BLOCK, 256), lambda i: (i, 0)),
            pl.BlockSpec((8, BLOCK), lambda i: (0, i)),
            whole(BLOCK + 16, 256),
            whole(BLOCK + 16, 256),
        ],
        out_shape=[
            jax.ShapeDtypeStruct((length, 512), F32),
            jax.ShapeDtypeStruct((length, 256), BF16),
            jax.ShapeDtypeStruct((8, length), F32),
            jax.ShapeDtypeStruct((BLOCK + 16, 256), BF16),
            jax.ShapeDtypeStruct((BLOCK + 16, 256), BF16),
        ],
        scratch_shapes=[
            pltpu.VMEM((BLOCK + 8, 1024), F32),
            pltpu.VMEM((2, 2 * BLOCK, 128), F32),
            pltpu.VMEM((2, 8, BLOCK), F32),
            pltpu.VMEM((BLOCK, 512), F32),
            pltpu.VMEM((8, BLOCK), F32),
            pltpu.VMEM((8, 512), F32),
        ],
        name="mixer",
        cost_estimate=cost(11),
    )(core, small_decay, large_decay, halo, small, large, keys, queries, small_step, large_step, small_taps, large_taps, key_taps, query_taps)


def chip_body(core, keep, other, out):
    own, far = get_state(keep[...]), get_state(other[...])
    first = core[0] == 0
    early = [jnp.where(first, a, b) for a, b in zip(own, far)]
    late = [jnp.where(first, b, a) for a, b in zip(own, far)]
    put_state(out, *then(early, late))


def chip_state(core, keep, other):
    return pl.pallas_call(
        chip_body,
        in_specs=[pl.BlockSpec(memory_space=pltpu.SMEM)] + [pl.BlockSpec()] * 2,
        out_shape=jax.ShapeDtypeStruct(keep.shape, BF16),
        name="chip_state",
        cost_estimate=cost(1),
    )(core, keep, other)


def line_body(position, own, back1, back2, back3, total, inside, held):
    for back, ref in enumerate((own, back1, back2, back3)):
        held[(position[0] + 4 - back) % 4] = ref[...]
    inside[...] = jnp.zeros_like(inside)
    prefix = None
    for j in range(4):
        piece = get_state(held[j])
        if prefix is None:
            prefix = piece
        else:
            prefix = then(prefix, piece)

        @pl.when(position[0] == j + 1)
        def _():
            inside[0:BLOCK, :] = prefix[0]
            inside[BLOCK : BLOCK + 8, :] = prefix[1]

    put_state(total, *prefix)


def line_state(position, *pieces):
    shape = pieces[0].shape
    return pl.pallas_call(
        line_body,
        in_specs=[pl.BlockSpec(memory_space=pltpu.SMEM)] + [pl.BlockSpec()] * 4,
        out_shape=[
            jax.ShapeDtypeStruct(shape, BF16),
            jax.ShapeDtypeStruct((BLOCK + 8, shape[1]), F32),
        ],
        scratch_shapes=[pltpu.VMEM((4, *shape), BF16)],
        name="line_state",
        cost_estimate=cost(1),
    )(position, *pieces)


def entering_body(core, inside, back1, back2, back3, keep, other, mine, send):
    held = get_state(back3[...])
    held = then(held, get_state(back2[...]))
    held = then(held, get_state(back1[...]))
    held = then(held, (inside[0:BLOCK, :], inside[BLOCK : BLOCK + 8, :]))
    own, far = get_state(keep[...]), get_state(other[...])
    first = core[0] == 0
    early = [jnp.where(first, a, b) for a, b in zip(own, far)]
    second = then(held, early)
    mine[...] = jnp.where(first, held[0], second[0]).astype(BF16)
    send[...] = jnp.where(first, second[0], held[0]).astype(BF16)


def entering_state(core, inside, back1, back2, back3, keep, other):
    shape = jax.ShapeDtypeStruct((BLOCK, keep.shape[1]), BF16)
    return pl.pallas_call(
        entering_body,
        in_specs=[pl.BlockSpec(memory_space=pltpu.SMEM)] + [pl.BlockSpec()] * 6,
        out_shape=[shape, shape],
        name="entering",
        cost_estimate=cost(1),
    )(core, inside, back1, back2, back3, keep, other)


def gate_body(core, mix, query, cum, mine, other, small_gate, large_gate, small_gain, large_gain, out):
    first = core[0] == 0
    entering = [jnp.where(first, mine[...], other[...]), jnp.where(first, other[...], mine[...])]
    cum_t = cum[...].T
    cum_cols = column_pairs([jnp.broadcast_to(cum_t[:, h : h + 1], (BLOCK, BLOCK)) for h in range(6)])
    q = query[...]
    carried = jnp.concatenate(
        [
            jnp.dot(q[:, 128 * g : 128 * g + 128], entering[g], preferred_element_type=F32)
            for g in range(2)
        ],
        axis=1,
    )
    y = mix[...] + carried * jnp.exp(cum_cols)
    lane = lax.broadcasted_iota(jnp.int32, (BLOCK, 128), 1)
    low = lane < 64
    for n in range(4):
        gate = (small_gate if n < 2 else large_gate)[:, 128 * (n % 2) : 128 * (n % 2) + 128].astype(F32)
        gain = (small_gain if n < 2 else large_gain)[:, 128 * (n % 2) : 128 * (n % 2) + 128].astype(F32)
        gated = y[:, 128 * n : 128 * n + 128] * (gate * jax.nn.sigmoid(gate))
        square = gated * gated
        if n < 2:
            first = jnp.sum(jnp.where(low, square, 0.0), axis=1, keepdims=True)
            second = jnp.sum(jnp.where(low, 0.0, square), axis=1, keepdims=True)
            scale = jnp.where(low, lax.rsqrt(first / 64 + EPS), lax.rsqrt(second / 64 + EPS))
        else:
            scale = lax.rsqrt(jnp.sum(square, axis=1, keepdims=True) / 128 + EPS)
        out[:, 128 * n : 128 * n + 128] = (gated * scale * gain).astype(BF16)


def gated_heads(part, parts, core, mix, query, cum, mine, other, small_gate, large_gate, small_gain, large_gain):
    length = mix.shape[0]
    whole = lambda *shape: pl.BlockSpec(shape, lambda i: (0,) * len(shape))
    rows = lambda width: pl.BlockSpec((BLOCK, width), lambda i: (parts * i + part, 0))
    return pl.pallas_call(
        gate_body,
        grid=(length // BLOCK // parts,),
        in_specs=[
            pl.BlockSpec(memory_space=pltpu.SMEM),
            rows(512),
            rows(256),
            pl.BlockSpec((8, BLOCK), lambda i: (0, parts * i + part)),
            whole(BLOCK, 256),
            whole(BLOCK, 256),
            rows(256),
            rows(256),
            whole(1, 256),
            whole(1, 256),
        ],
        out_specs=pl.BlockSpec((BLOCK, 512), lambda i: (i, 0)),
        out_shape=jax.ShapeDtypeStruct((length // parts, 512), BF16),
        name="gated",
        cost_estimate=cost(4),
    )(core, mix, query, cum, mine, other, small_gate, large_gate, small_gain, large_gain)


SHARES = 4
WIDE_COLS = 256


def project_body(
    core, place, own, left, right, diag_low, diag_high,
    small_out, large_out, near_left, far_left, near_right, far_right, near_diag, far_diag,
    residual, mixer_gain, ffn_gain, normed_out, mixed_out, heads, acc,
):
    step = pl.program_id(0)
    width = own.shape[1] // 2
    rows = own.shape[0]

    @pl.when(step == 0)
    def _():
        heads[:, 0 : 2 * width] = own[...]
        first = core[0] == 0
        half = rows // 2
        parts = (
            (left, 0, rows, 1),
            (right, 0, rows, 2),
            (diag_low, 0, half, 3),
            (diag_high, half, rows, 3),
        )
        for ref, begin, end, n in parts:
            small, large = ref[:, 0:width], ref[:, width:]
            at = 2 * width * n
            heads[begin:end, at : at + width] = jnp.where(first, small, large)
            heads[begin:end, at + width : at + 2 * width] = jnp.where(first, large, small)

    weights = (small_out, large_out, near_left, far_left, near_right, far_right, near_diag, far_diag)
    out = jnp.dot(heads[:, 0:width], weights[0][...], preferred_element_type=F32)
    for n in range(1, 8):
        out = out + jnp.dot(heads[:, n * width : (n + 1) * width], weights[n][...], preferred_element_type=F32)
    acc[:, pl.ds(pl.multiple_of(step * WIDE_COLS, WIDE_COLS), WIDE_COLS)] = out

    @pl.when(step == pl.num_programs(0) - 1)
    def _():
        share = rows // SHARES
        few = 16
        for n, ahead in enumerate((0, 1, 3, 2)):
            at = (place[0] + ahead) % SHARES

            def one(k, _):
                mix = acc[pl.ds(pl.multiple_of(at * share + k * few, few), few), :]
                scale = lax.rsqrt(jnp.mean(mix * mix, axis=1, keepdims=True) + EPS)
                mixed = residual[at, 0, pl.ds(pl.multiple_of(k * few, few), few), :].astype(F32)
                mixed = mixed + mix * scale * mixer_gain[...].astype(F32)
                scale = lax.rsqrt(jnp.mean(mixed * mixed, axis=1, keepdims=True) + EPS)
                normed = mixed * scale * ffn_gain[...].astype(F32)
                normed_out[pl.ds(pl.multiple_of(n * share + k * few, few), few), :] = normed.astype(BF16)
                if n == 0:
                    mixed_out[pl.ds(pl.multiple_of(k * few, few), few), :] = mixed
                return 0

            lax.fori_loop(0, share // few, one, 0)


def project(part, parts, core, place, pieces, weights, residual, mixer_gain, ffn_gain):
    rows = pieces[0].shape[0]
    features = residual.shape[1]
    share = rows // SHARES
    whole = lambda a: pl.BlockSpec(a.shape, lambda i: (0, 0))
    return pl.pallas_call(
        project_body,
        grid=(features // WIDE_COLS,),
        in_specs=[pl.BlockSpec(memory_space=pltpu.SMEM)] * 2
        + [whole(p) for p in pieces]
        + [pl.BlockSpec((w.shape[0], WIDE_COLS), lambda i: (0, i)) for w in weights]
        + [
            pl.BlockSpec((SHARES, 1, share, features), lambda i: (0, part, 0, 0)),
            whole(mixer_gain),
            whole(ffn_gain),
        ],
        out_specs=[
            pl.BlockSpec((rows, features), lambda i: (0, 0)),
            pl.BlockSpec((share, features), lambda i: (0, 0)),
        ],
        out_shape=[
            jax.ShapeDtypeStruct((rows, features), BF16),
            jax.ShapeDtypeStruct((share, features), F32),
        ],
        scratch_shapes=[pltpu.VMEM((rows, features), BF16), pltpu.VMEM((rows, features), F32)],
        name="project",
        cost_estimate=cost(7),
    )(core, place, *pieces, *weights, residual.reshape(SHARES, parts, share, features), mixer_gain, ffn_gain)


def channel_body(x, proj, down, own, right, left, diag_low, diag_high, acc, hidden):
    step = pl.program_id(0)
    wide = hidden.shape[1]
    rows = x.shape[0]
    share = rows // SHARES

    @pl.when(step == 0)
    def _():
        acc[...] = jnp.dot(x[...], proj[...], preferred_element_type=F32)

    @pl.when(jnp.logical_and(step > 0, step < 4))
    def _():
        acc[...] += jnp.dot(x[...], proj[...], preferred_element_type=F32)

    @pl.when(step == 3)
    def _():
        few = 16

        def one(k, _):
            at = pl.ds(pl.multiple_of(k * few, few), few)
            gate = acc[at, 0:wide]
            hidden[at, :] = (gate * jax.nn.sigmoid(gate) * acc[at, wide:]).astype(BF16)
            return 0

        lax.fori_loop(0, rows // few, one, 0)

    @pl.when(step >= 4)
    def _():
        out = lax.dot_general(
            hidden[...], down[...], (((1,), (1,)), ((), ())), preferred_element_type=F32
        ).astype(BF16)
        own[...] = out[0:share]
        right[...] = out[share : 2 * share]
        left[...] = out[2 * share : 3 * share]
        diag_low[...] = out[3 * share : 3 * share + share // 2]
        diag_high[...] = out[3 * share + share // 2 :]


def channel(x, whole_proj):
    rows, features = x.shape
    wide = whole_proj.shape[1] // 3
    share = rows // SHARES
    deep = features // 4
    heights = (share, share, share, share // 2, share // 2)
    return pl.pallas_call(
        channel_body,
        grid=(8,),
        in_specs=[
            pl.BlockSpec((rows, deep), lambda i: (0, jnp.minimum(i, 3))),
            pl.BlockSpec((deep, 2 * wide), lambda i: (jnp.minimum(i, 3), 0)),
            pl.BlockSpec((deep, wide), lambda i: (jnp.maximum(i - 4, 0), 2)),
        ],
        out_specs=[pl.BlockSpec((h, deep), lambda i: (0, jnp.maximum(i - 4, 0))) for h in heights],
        out_shape=[jax.ShapeDtypeStruct((h, features), BF16) for h in heights],
        scratch_shapes=[pltpu.VMEM((rows, 2 * wide), F32), pltpu.VMEM((rows, wide), BF16)],
        name="channel",
        cost_estimate=cost(12),
    )(x, whole_proj, whole_proj)


def add_body(right, from_left, left, from_right, right_out, left_out):
    half = from_left.shape[0]
    right_out[half:, :] = right[half:, :]
    right_out[:half, :] = (right[:half, :].astype(F32) + from_left[...].astype(F32)).astype(BF16)
    left_out[:half, :] = left[:half, :]
    left_out[half:, :] = (left[half:, :].astype(F32) + from_right[...].astype(F32)).astype(BF16)


def add_passing(right, from_left, left, from_right):
    return pl.pallas_call(
        add_body,
        out_shape=[jax.ShapeDtypeStruct(right.shape, BF16), jax.ShapeDtypeStruct(left.shape, BF16)],
        name="add_passing",
        cost_estimate=cost(1),
    )(right, from_left, left, from_right)


def finish_body(*refs):
    *parts, gain, out = refs
    share = parts[0].shape[0]
    few = 16
    for n in range(len(parts) // 4):
        own, one_side, other_side, mixed = parts[4 * n : 4 * n + 4]

        def one(k, _):
            at = pl.ds(pl.multiple_of(k * few, few), few)
            ffn = own[at, :].astype(F32) + one_side[at, :].astype(F32) + other_side[at, :].astype(F32)
            scale = 0.5 * lax.rsqrt(jnp.mean(ffn * ffn, axis=1, keepdims=True) + EPS)
            done = mixed[at, :] + ffn * scale * gain[...].astype(F32)
            out[pl.ds(pl.multiple_of(n * share + k * few, few), few), :] = done.astype(BF16)
            return 0

        lax.fori_loop(0, share // few, one, 0)


def finish(parts, gain):
    share, features = parts[0][0].shape
    flat = [a for part in parts for a in part]
    return pl.pallas_call(
        finish_body,
        out_shape=jax.ShapeDtypeStruct((len(parts) * share, features), BF16),
        name="finish",
        cost_estimate=cost(3),
    )(*flat, gain)


SP = ("sp_0", "sp_1", "sp_2")
SP_TP = ("sp_0", "sp_1", "sp_2", "tp")


PARTS = 2


def turned(axis, distance):
    size = lax.axis_size(axis)
    return [(i, (i + distance) % size) for i in range(size)]


def onward(axis, distance):
    size = lax.axis_size(axis)
    return [(i, i + distance) for i in range(size - distance)]


def round_line(array, axis):
    half = array.shape[0] // 2
    left = lax.ppermute(array, axis, turned(axis, 1))
    right = lax.ppermute(array, axis, turned(axis, -1))
    low = lax.ppermute(left[:half], axis, turned(axis, 1))
    high = lax.ppermute(right[half:], axis, turned(axis, -1))
    return [array, left, right, low, high]


def scalar(value):
    return value.astype(jnp.int32).reshape(1)


def local(
    residual,
    small_heads,
    large_heads,
    state_keys,
    state_queries,
    small_gate,
    large_gate,
    small_step,
    large_step,
    small_taps,
    large_taps,
    key_taps,
    query_taps,
    small_decay,
    large_decay,
    small_gain,
    large_gain,
    small_out,
    large_out,
    mixer_gain,
    ffn_in_gain,
    gate_proj,
    up_proj,
    down_proj,
    ffn_out_gain,
):
    length = residual.shape[0]
    wide = gate_proj.shape[1]
    whole_proj = lax.all_gather(
        jnp.concatenate([gate_proj, up_proj, down_proj], axis=1), SP, axis=0, tiled=True
    )
    keys = state_keys.reshape(2 * length, 128)
    queries = state_queries.reshape(2 * length, 128)
    devices = range(lax.axis_size(SP))
    halo = lax.ppermute(
        pack_halo(small_heads, large_heads, keys, queries), SP, [(i, i + 1) for i in devices[:-1]]
    )
    core = scalar(lax.axis_index("sp_2"))
    place = scalar(lax.axis_index("tp"))
    mix, query_conv, cum, keep, send = mixer(
        core,
        halo,
        small_heads,
        large_heads,
        keys,
        queries,
        small_step.T,
        large_step.T,
        small_taps,
        large_taps,
        key_taps.reshape(8, 128),
        query_taps.reshape(8, 128),
        small_decay,
        large_decay,
    )
    near = jnp.where(core == 0, small_out, large_out)
    near_out = [lax.ppermute(near, "tp", turned("tp", d)) for d in (1, -1, 2)]
    far_out = [lax.ppermute(a, "sp_2", turned("sp_2", 1)) for a in near_out]
    out_weights = [small_out, large_out]
    for a, b in zip(near_out, far_out):
        out_weights += [a, b]

    other = lax.ppermute(send, "sp_2", turned("sp_2", 1))
    chip = chip_state(core, keep, other)
    line, inside = line_state(
        scalar(lax.axis_index("sp_1")),
        chip,
        *[lax.ppermute(chip, "sp_1", turned("sp_1", d)) for d in (1, 2, 3)],
    )
    mine, send = entering_state(
        core, inside, *[lax.ppermute(line, "sp_0", onward("sp_0", d)) for d in (1, 2, 3)], keep, other
    )
    theirs = lax.ppermute(send, "sp_2", turned("sp_2", 1))

    parts = []
    for part in range(PARTS):
        normed = gated_heads(
            part,
            PARTS,
            core,
            mix,
            query_conv,
            cum,
            mine,
            theirs,
            small_gate,
            large_gate,
            small_gain.reshape(1, -1),
            large_gain.reshape(1, -1),
        )
        pieces = round_line(normed, "tp")
        normed_in, mixed = project(
            part,
            PARTS,
            core,
            place,
            pieces,
            out_weights,
            residual,
            mixer_gain.reshape(1, -1),
            ffn_in_gain.reshape(1, -1),
        )
        own, right, left, low, high = channel(normed_in, whole_proj)
        low = lax.ppermute(low, "tp", turned("tp", 1))
        high = lax.ppermute(high, "tp", turned("tp", -1))
        right, left = add_passing(right, low, left, high)
        parts.append(
            (
                own,
                lax.ppermute(right, "tp", turned("tp", 1)),
                lax.ppermute(left, "tp", turned("tp", -1)),
                mixed,
            )
        )
    return finish(parts, ffn_out_gain.reshape(1, -1))


def solution(mesh):
    torus = Mesh(mesh.devices.reshape(4, 4, 2, mesh.shape["tp"]), ("sp_0", "sp_1", "sp_2", "tp"))
    in_specs = (
        P(SP, None),
        P(SP, "tp"),
        P(SP, "tp"),
        P(SP, "tp", None),
        P(SP, "tp", None),
        P(SP, "tp"),
        P(SP, "tp"),
        P(SP, "tp"),
        P(SP, "tp"),
        P(None, "tp"),
        P(None, "tp"),
        P(None, "tp", None),
        P(None, "tp", None),
        P("tp"),
        P("tp"),
        P("tp"),
        P("tp"),
        P("tp", None),
        P("tp", None),
        P(),
        P(),
        P(SP, "tp"),
        P(SP, "tp"),
        P(SP, "tp"),
        P(),
    )
    out_specs = P(SP_TP, None)
    return jax.shard_map(local, mesh=torus, in_specs=in_specs, out_specs=out_specs, check_vma=False)
```

time: 490 us -> 237 us (0.48)
  local copies, waits for them, and re-layouts: 137 us -> 12.7 us
  Pallas kernels: 0 us -> 108 us
  matrix products: 104 us -> 0 us
  waiting for transfers between devices: 143 us -> 42.2 us
  other arithmetic: 45 us -> 3.18 us
  starting transfers between devices: 12.4 us -> 53.3 us
  blocking collectives: 24.6 us -> 0 us
    pallas_call x0 -> x14, Pallas kernels: none -> 108 us  [the longest x2 38.7 us: project(): pl.pallas_call(project_body, grid=(features // WIDE_COLS,), in_specs=[pl....]
    dot_general x70 -> x0, matrix products: 104 us -> none  [the longest x1 21.5 us: local(): lax.dot_general(hidden, down_full, (((1,), (1,)), ((), ())), preferred_el...]
    psum x1 -> x0, waiting for transfers between devices: 94.6 us -> none  [local(): mix = lax.psum(partial_value.astype(jnp.bfloat16), 'tp').astype(jnp.float32)]
    dynamic_update_slice x32 -> x0, local copies, waits for them, and re-layouts: 83.5 us -> none  [block_pass(): end_state, (outputs, cumulative) = lax.scan(one_block, start_state, blocked)]
    reduce_scatter x1 -> x0, waiting for transfers between devices: 46.8 us -> none  [local(): lax.psum_scatter(lax.dot_general(hidden, down_full, (((1,), (1,)), ((), (...]
    ppermute x4 -> x31, waiting for transfers between devices: 0.01 us -> 42.1 us  [the longest x2 15.5 us: round_line(): left = lax.ppermute(array, axis, turned(axis, 1))]
    ppermute x4 -> x31, starting transfers between devices: 12 us -> 53.3 us  [the longest x3 13 us: local(): lax.ppermute(line, 'sp_0', onward('sp_0', d))]
    all_gather x3 -> x0, blocking collectives: 24.6 us -> none  [collected_together(): both, at, found = (lax.all_gather(jnp.concatenate(lines), axis), 0, {})]
  transfers between devices with their start and end apart: 9 -> 32, of which waited for: 2 -> 10; matrix products, arithmetic and copies ran while one was open for 51% -> 3% of each run, Pallas kernels for 0% -> 37%
where the time goes in v1:
time: 237 us; the launch traced here: 233 us
  Pallas kernels  108 us (46%)
  starting transfers between devices  53.3 us (22%)
  waiting for transfers between devices  42.2 us (18%)
  between operations  13.7 us (6%)
  local copies, waits for them, and re-layouts  12.7 us (5%)
  other arithmetic  3.18 us (1%)
    pallas_call x2, Pallas kernels, project(): pl.pallas_call(project_body, grid=(features // WIDE_COLS,), in_specs=[pl....  38.7 us
    pallas_call x2, Pallas kernels, channel(): pl.pallas_call(channel_body, grid=(8,), in_specs=[pl.BlockSpec((rows, dee...  32.4 us
    ppermute x2, waiting for transfers between devices, round_line(): left = lax.ppermute(array, axis, turned(axis, 1))  15.5 us
    ppermute x2, waiting for transfers between devices, local(): lax.ppermute(right, 'tp', turned('tp', 1))  15 us
    ppermute x3, starting transfers between devices, local(): lax.ppermute(line, 'sp_0', onward('sp_0', d))  13 us
    pallas_call x1, Pallas kernels, mixer(): pl.pallas_call(mixer_body, grid=(blocks,), in_specs=[pl.BlockSpec(memory_...  10.7 us
    pallas_call x2, Pallas kernels, gated_heads(): pl.pallas_call(gate_body, grid=(length // BLOCK // parts,), in_specs=[pl....  9.32 us
    unnamed x60, local copies, waits for them, and re-layouts  6.39 us
  transfers between devices with their start and end apart: 32, of which 10 were waited for; matrix products, arithmetic and copies ran while one was open for 3% of the time, Pallas kernels for 37%

profile of v1, /device:TPU:1, one launch (start us, length us, event | category | flops | bytes accessed | tf_op | source)
XLA Modules:
  0.0 233.1 jit_solution(14257886236971287739)
XLA Ops:
  10.0 4.6 %collective-permute-start = (bf16[16,1024]{1,0:T(8,128)(2,1)}, bf16[16,1024]{1,0:T(8,128)(2,1)S(1)}, u32[]{:S(2)}, u32[]{:S(2)}) collective-permute-start(bf16[16,1024]{1,0:T(8,128)(2,1)} %pack_halo.1), channel_id=1, source_target_pairs={{0,4},{4,8},{8,12},{12,16},{16,20},{20,24},{24,28},{28,32},{32,36}... | collective-permute-start | bytes 98312 | tf_op jit(solution)/shard_map/ppermute | solution.py:658
  20.5 10.7 %mixer.1 = (f32[1024,512]{1,0:T(8,128)}, bf16[1024,256]{1,0:T(8,128)(2,1)}, f32[8,1024]{1,0:T(8,128)}, bf16[144,256]{1,0:T(8,128)(2,1)}, bf16[144,256]{1,0:T(8,128)(2,1)}) custom-call(s32[1]{0:T(128)} %bitcast.core, f32[4]{0:T(128)} %small_decay.1, f32[2]{0:T(128)} %large_decay.1, bf16[16,1024]{1,0:T(8,128)(2,1)} %copy-done.27, bf16[1024,256]{1,0:T(8,128)(2,1)} %small.3, ...), custom_call_target="tpu_custom_call" | custom-call | flops 2750000128 | bytes 1100000 | tf_op jit(solution)/shard_map/mixer/pallas_call | solution.py:220
  46.4 3.6 %collective-permute-start.5 = (bf16[144,256]{1,0:T(8,128)(2,1)}, bf16[144,256]{1,0:T(8,128)(2,1)S(1)}, u32[]{:S(2)}, u32[]{:S(2)}) collective-permute-start(bf16[144,256]{1,0:T(8,128)(2,1)} %get-tuple-element.38), channel_id=1, source_target_pairs={{0,32},{32,64},{64,96},{1,33},{33,65},{65,97},{2,34},{34,66},{66,9... | collective-permute-start | bytes 221192 | tf_op jit(solution)/shard_map/ppermute | solution.py:694
  50.0 5.1 %collective-permute-start.6 = (bf16[144,256]{1,0:T(8,128)(2,1)}, bf16[144,256]{1,0:T(8,128)(2,1)S(1)}, u32[]{:S(2)}, u32[]{:S(2)}) collective-permute-start(bf16[144,256]{1,0:T(8,128)(2,1)} %get-tuple-element.38), channel_id=1, source_target_pairs={{0,64},{32,96},{1,65},{33,97},{2,66},{34,98},{3,67},{35,99},{4,68}... | collective-permute-start | bytes 221192 | tf_op jit(solution)/shard_map/ppermute | solution.py:694
  55.1 4.3 %collective-permute-start.7 = (bf16[144,256]{1,0:T(8,128)(2,1)}, bf16[144,256]{1,0:T(8,128)(2,1)S(1)}, u32[]{:S(2)}, u32[]{:S(2)}) collective-permute-start(bf16[144,256]{1,0:T(8,128)(2,1)} %get-tuple-element.38), channel_id=1, source_target_pairs={{0,96},{1,97},{2,98},{3,99},{4,100},{5,101},{6,102},{7,103},{8,104... | collective-permute-start | bytes 221192 | tf_op jit(solution)/shard_map/ppermute | solution.py:694
  59.4 3.3 %collective-permute-done.7.back3 = bf16[144,256]{1,0:T(8,128)(2,1)S(1)} collective-permute-done((bf16[144,256]{1,0:T(8,128)(2,1)}, bf16[144,256]{1,0:T(8,128)(2,1)S(1)}, u32[]{:S(2)}, u32[]{:S(2)}) %collective-permute-start.7) | collective-permute-done | bytes 73760 | tf_op jit(solution)/shard_map/ppermute | solution.py:694
  65.1 3.5 %collective-permute-start.8 = (bf16[128,256]{1,0:T(8,128)(2,1)}, bf16[128,256]{1,0:T(8,128)(2,1)S(1)}, u32[]{:S(2)}, u32[]{:S(2)}) collective-permute-start(bf16[128,256]{1,0:T(8,128)(2,1)} %get-tuple-element.40), channel_id=1, source_target_pairs={{0,4},{4,0},{1,5},{5,1},{2,6},{6,2},{3,7},{7,3},{8,12},{12,8},{9,1... | collective-permute-start | bytes 196616 | tf_op jit(solution)/shard_map/ppermute | solution.py:696
  70.5 4.6 %gated.3.own = bf16[512,512]{1,0:T(8,128)(2,1)} custom-call(s32[1]{0:T(128)} %bitcast.core, f32[1024,512]{1,0:T(8,128)} %get-tuple-element.32.mix, bf16[1024,256]{1,0:T(8,128)(2,1)} %get-tuple-element.33.query, f32[8,1024]{1,0:T(8,128)} %get-tuple-element.34.cum, bf16[128,256]{1,0:T(8,128)(2,1)} %get-tuple-element.39.mine, bf16[128,256]{1,0:T(8,128)(2,1)} %copy-done.12, ...), custom_call_target="tpu_custom_call" | custom-call | flops 1000000000 | bytes 400000 | tf_op jit(solution)/shard_map/gated/pallas_call | solution.py:377
  79.0 4.7 %gated.2.own = bf16[512,512]{1,0:T(8,128)(2,1)} custom-call(s32[1]{0:T(128)} %bitcast.core, f32[1024,512]{1,0:T(8,128)} %get-tuple-element.32.mix, bf16[1024,256]{1,0:T(8,128)(2,1)} %get-tuple-element.33.query, f32[8,1024]{1,0:T(8,128)} %get-tuple-element.34.cum, bf16[128,256]{1,0:T(8,128)(2,1)} %get-tuple-element.39.mine, bf16[128,256]{1,0:T(8,128)(2,1)} %copy-done.12, ...), custom_call_target="tpu_custom_call" | custom-call | flops 1000000000 | bytes 400000 | tf_op jit(solution)/shard_map/gated/pallas_call | solution.py:377
  83.7 6.2 %collective-permute-done.23.left = bf16[512,512]{1,0:T(8,128)(2,1)} collective-permute-done((bf16[512,512]{1,0:T(8,128)(2,1)}, bf16[512,512]{1,0:T(8,128)(2,1)}, u32[]{:S(2)}, u32[]{:S(2)}) %collective-permute-start.23) | collective-permute-done | bytes 524320 | tf_op jit(solution)/shard_map/ppermute | solution.py:612
  90.0 2.7 %collective-permute-start.10 = (bf16[512,512]{1,0:T(8,128)(2,1)}, bf16[512,512]{1,0:T(8,128)(2,1)S(1)}, u32[]{:S(2)}, u32[]{:S(2)}) collective-permute-start(bf16[512,512]{1,0:T(8,128)(2,1)} %gated.2.own), channel_id=1, source_target_pairs={{0,3},{1,0},{2,1},{3,2},{4,7},{5,4},{6,5},{7,6},{8,11},{9,8},{10,9... | collective-permute-start | bytes 1572872 | tf_op jit(solution)/shard_map/ppermute | solution.py:613
  94.6 9.3 %collective-permute-done.9.left = bf16[512,512]{1,0:T(8,128)(2,1)S(1)} collective-permute-done((bf16[512,512]{1,0:T(8,128)(2,1)}, bf16[512,512]{1,0:T(8,128)(2,1)S(1)}, u32[]{:S(2)}, u32[]{:S(2)}) %collective-permute-start.9) | collective-permute-done | bytes 524320 | tf_op jit(solution)/shard_map/ppermute | solution.py:612
  108.0 3.2 %collective-permute-done.25.diag_low = bf16[256,512]{1,0:T(8,128)(2,1)} collective-permute-done((bf16[256,512]{1,0:T(8,128)(2,1)S(1)}, bf16[256,512]{1,0:T(8,128)(2,1)}, u32[]{:S(2)}, u32[]{:S(2)}) %collective-permute-start.25) | collective-permute-done | bytes 262176 | tf_op jit(solution)/shard_map/ppermute | solution.py:614
  111.3 2.7 %collective-permute-start.12 = (bf16[256,512]{1,0:T(8,128)(2,1)}, bf16[256,512]{1,0:T(8,128)(2,1)}, u32[]{:S(2)}, u32[]{:S(2)}) collective-permute-start(bf16[256,512]{1,0:T(8,128)(2,1)} %slice.17), channel_id=1, source_target_pairs={{0,3},{1,0},{2,1},{3,2},{4,7},{5,4},{6,5},{7,6},{8,11},{9,8},{10,9... | collective-permute-start | bytes 786440 | tf_op jit(solution)/shard_map/ppermute | solution.py:615
  115.1 19.4 %project.3 = (bf16[512,2048]{1,0:T(8,128)(2,1)}, f32[128,2048]{1,0:T(8,128)}) custom-call(s32[1]{0:T(128)} %bitcast.core, s32[1]{0:T(128)} %bitcast.1.place, bf16[512,512]{1,0:T(8,128)(2,1)} %gated.3.own, bf16[512,512]{1,0:T(8,128)(2,1)} %collective-permute-done.23.left, bf16[512,512]{1,0:T(8,128)(2,1)} %collective-permute-done.24.right, ...), custom_call_target="tpu_custom_call" | custom-call | flops 1750000000 | bytes 700000 | tf_op jit(solution)/shard_map/project/pallas_call | solution.py:462
  135.2 19.3 %project.2 = (bf16[512,2048]{1,0:T(8,128)(2,1)}, f32[128,2048]{1,0:T(8,128)}) custom-call(s32[1]{0:T(128)} %bitcast.core, s32[1]{0:T(128)} %bitcast.1.place, bf16[512,512]{1,0:T(8,128)(2,1)} %gated.2.own, bf16[512,512]{1,0:T(8,128)(2,1)} %copy-done.5, bf16[512,512]{1,0:T(8,128)(2,1)} %copy-done.6, bf16[256,512]{1,0:T(8,128)(2,1)} %copy-done.11, ...), custom_call_target="tpu_custom_call" | custom-call | flops 1750000000 | bytes 700000 | tf_op jit(solution)/shard_map/project/pallas_call | solution.py:462
  154.6 16.2 %channel.3 = (bf16[128,2048]{1,0:T(8,128)(2,1)}, bf16[128,2048]{1,0:T(8,128)(2,1)}, bf16[128,2048]{1,0:T(8,128)(2,1)}, bf16[64,2048]{1,0:T(8,128)(2,1)}, bf16[64,2048]{1,0:T(8,128)(2,1)}) custom-call(bf16[512,2048]{1,0:T(8,128)(2,1)} %get-tuple-element.50.x, bf16[2048,4224]{1,0:T(8,128)(2,1)} %all-gather.2.cloned.1.call-done.proj.down, ...), custom_call_target="tpu_custom_call" | custom-call | flops 3000000000 | bytes 1200000 | tf_op jit(solution)/shard_map/channel/pallas_call | solution.py:531
  170.8 2.7 %collective-permute-start.28 = (bf16[64,2048]{1,0:T(8,128)(2,1)}, bf16[64,2048]{1,0:T(8,128)(2,1)S(1)}, u32[]{:S(2)}, u32[]{:S(2)}) collective-permute-start(bf16[64,2048]{1,0:T(8,128)(2,1)} %get-tuple-element.55), channel_id=1, source_target_pairs={{0,3},{1,0},{2,1},{3,2},{4,7},{5,4},{6,5},{7,6},{8,11},{9,8},{10,9... | collective-permute-start | bytes 786440 | tf_op jit(solution)/shard_map/ppermute | solution.py:728
  173.5 16.1 %channel.2 = (bf16[128,2048]{1,0:T(8,128)(2,1)}, bf16[128,2048]{1,0:T(8,128)(2,1)}, bf16[128,2048]{1,0:T(8,128)(2,1)}, bf16[64,2048]{1,0:T(8,128)(2,1)}, bf16[64,2048]{1,0:T(8,128)(2,1)}) custom-call(bf16[512,2048]{1,0:T(8,128)(2,1)} %get-tuple-element.41.x, bf16[2048,4224]{1,0:T(8,128)(2,1)} %all-gather.2.cloned.1.call-done.proj.down, ...), custom_call_target="tpu_custom_call" | custom-call | flops 3000000000 | bytes 1200000 | tf_op jit(solution)/shard_map/channel/pallas_call | solution.py:531
  195.6 2.7 %collective-permute-start.30 = (bf16[128,2048]{1,0:T(8,128)(2,1)}, bf16[128,2048]{1,0:T(8,128)(2,1)S(1)}, u32[]{:S(2)}, u32[]{:S(2)}) collective-permute-start(bf16[128,2048]{1,0:T(8,128)(2,1)} %get-tuple-element.57), channel_id=1, source_target_pairs={{0,3},{1,0},{2,1},{3,2},{4,7},{5,4},{6,5},{7,6},{8,11},{9,8},{10,9... | collective-permute-start | bytes 1572872 | tf_op jit(solution)/shard_map/ppermute | solution.py:734
  201.5 2.7 %collective-permute-start.22 = (bf16[128,2048]{1,0:T(8,128)(2,1)}, bf16[128,2048]{1,0:T(8,128)(2,1)S(1)}, u32[]{:S(2)}, u32[]{:S(2)}) collective-permute-start(bf16[128,2048]{1,0:T(8,128)(2,1)} %get-tuple-element.48), channel_id=1, source_target_pairs={{0,3},{1,0},{2,1},{3,2},{4,7},{5,4},{6,5},{7,6},{8,11},{9,8},{10,9... | collective-permute-start | bytes 1572872 | tf_op jit(solution)/shard_map/ppermute | solution.py:734
  204.8 3.8 %collective-permute-done.29.refs_5_ = bf16[128,2048]{1,0:T(8,128)(2,1)S(1)} collective-permute-done((bf16[128,2048]{1,0:T(8,128)(2,1)}, bf16[128,2048]{1,0:T(8,128)(2,1)S(1)}, u32[]{:S(2)}, u32[]{:S(2)}) %collective-permute-start.29) | collective-permute-done | bytes 524320 | tf_op jit(solution)/shard_map/ppermute | solution.py:733
  208.5 11.2 %collective-permute-done.21.refs_1_ = bf16[128,2048]{1,0:T(8,128)(2,1)S(1)} collective-permute-done((bf16[128,2048]{1,0:T(8,128)(2,1)}, bf16[128,2048]{1,0:T(8,128)(2,1)S(1)}, u32[]{:S(2)}, u32[]{:S(2)}) %collective-permute-start.21) | collective-permute-done | bytes 524320 | tf_op jit(solution)/shard_map/ppermute | solution.py:733
  220.7 5.5 %finish.1 = bf16[256,2048]{1,0:T(8,128)(2,1)} custom-call(bf16[128,2048]{1,0:T(8,128)(2,1)} %get-tuple-element.42.refs_0_, bf16[128,2048]{1,0:T(8,128)(2,1)} %copy-done.9, bf16[128,2048]{1,0:T(8,128)(2,1)} %copy-done.10, f32[128,2048]{1,0:T(8,128)} %get-tuple-element.49.refs_3_, bf16[128,2048]{1,0:T(8,128)(2,1)} %get-tuple-element.51.refs_4_, ...), custom_call_target="tpu_custom_call" | custom-call | flops 750000000 | bytes 300000 | tf_op jit(solution)/shard_map/finish/pallas_call | solution.py:585
  (126 shorter events, 51.4 us)
Async XLA Ops:
  6.5 148.0 %all-gather.2.cloned.1.call-start = ((), (), s32[]{:S(2)}) async-start(), calls=%async_computation | async-start | bytes 17842176 | tf_op jit(solution)/shard_map/all_gather | solution.py:652
  10.0 9.9 %collective-permute-start = (bf16[16,1024]{1,0:T(8,128)(2,1)}, bf16[16,1024]{1,0:T(8,128)(2,1)S(1)}, u32[]{:S(2)}, u32[]{:S(2)}) collective-permute-start(bf16[16,1024]{1,0:T(8,128)(2,1)} %pack_halo.1), channel_id=1, source_target_pairs={{0,4},{4,8},{8,12},{12,16},{16,20},{20,24},{24,28},{28,32},{32,36}... | collective-permute-start | bytes 98312 | tf_op jit(solution)/shard_map/ppermute | solution.py:658
  15.7 62.0 %collective-permute-start.13 = (bf16[256,2048]{1,0:T(8,128)(2,1)}, bf16[256,2048]{1,0:T(8,128)(2,1)S(1)}, u32[]{:S(2)}, u32[]{:S(2)}) collective-permute-start(bf16[256,2048]{1,0:T(8,128)(2,1)} %broadcast_select_fusion), channel_id=1, source_target_pairs={{0,1},{1,2},{2,3},{3,0},{4,5},{5,6},{6,7},{7,4},{8,9},{9,10},{10,1... | collective-permute-start | bytes 3145736 | tf_op jit(solution)/shard_map/ppermute | solution.py:680
  16.9 61.5 %collective-permute-start.15 = (bf16[256,2048]{1,0:T(8,128)(2,1)}, bf16[256,2048]{1,0:T(8,128)(2,1)S(1)}, u32[]{:S(2)}, u32[]{:S(2)}) collective-permute-start(bf16[256,2048]{1,0:T(8,128)(2,1)} %broadcast_select_fusion), channel_id=1, source_target_pairs={{0,3},{1,0},{2,1},{3,2},{4,7},{5,4},{6,5},{7,6},{8,11},{9,8},{10,9... | collective-permute-start | bytes 3145736 | tf_op jit(solution)/shard_map/ppermute | solution.py:680
  18.4 60.1 %collective-permute-start.17 = (bf16[256,2048]{1,0:T(8,128)(2,1)}, bf16[256,2048]{1,0:T(8,128)(2,1)S(1)}, u32[]{:S(2)}, u32[]{:S(2)}) collective-permute-start(bf16[256,2048]{1,0:T(8,128)(2,1)} %broadcast_select_fusion), channel_id=1, source_target_pairs={{0,2},{1,3},{2,0},{3,1},{4,6},{5,7},{6,4},{7,5},{8,10},{9,11},{10,... | collective-permute-start | bytes 3145736 | tf_op jit(solution)/shard_map/ppermute | solution.py:680
  46.4 8.7 %collective-permute-start.5 = (bf16[144,256]{1,0:T(8,128)(2,1)}, bf16[144,256]{1,0:T(8,128)(2,1)S(1)}, u32[]{:S(2)}, u32[]{:S(2)}) collective-permute-start(bf16[144,256]{1,0:T(8,128)(2,1)} %get-tuple-element.38), channel_id=1, source_target_pairs={{0,32},{32,64},{64,96},{1,33},{33,65},{65,97},{2,34},{34,66},{66,9... | collective-permute-start | bytes 221192 | tf_op jit(solution)/shard_map/ppermute | solution.py:694
  50.0 9.4 %collective-permute-start.6 = (bf16[144,256]{1,0:T(8,128)(2,1)}, bf16[144,256]{1,0:T(8,128)(2,1)S(1)}, u32[]{:S(2)}, u32[]{:S(2)}) collective-permute-start(bf16[144,256]{1,0:T(8,128)(2,1)} %get-tuple-element.38), channel_id=1, source_target_pairs={{0,64},{32,96},{1,65},{33,97},{2,66},{34,98},{3,67},{35,99},{4,68}... | collective-permute-start | bytes 221192 | tf_op jit(solution)/shard_map/ppermute | solution.py:694
  75.1 14.9 %collective-permute-start.23 = (bf16[512,512]{1,0:T(8,128)(2,1)}, bf16[512,512]{1,0:T(8,128)(2,1)}, u32[]{:S(2)}, u32[]{:S(2)}) collective-permute-start(bf16[512,512]{1,0:T(8,128)(2,1)} %gated.3.own), channel_id=1, source_target_pairs={{0,1},{1,2},{2,3},{3,0},{4,5},{5,6},{6,7},{7,4},{8,9},{9,10},{10,1... | collective-permute-start | bytes 1572872 | tf_op jit(solution)/shard_map/ppermute | solution.py:612
  75.3 14.7 %collective-permute-start.24 = (bf16[512,512]{1,0:T(8,128)(2,1)}, bf16[512,512]{1,0:T(8,128)(2,1)}, u32[]{:S(2)}, u32[]{:S(2)}) collective-permute-start(bf16[512,512]{1,0:T(8,128)(2,1)} %gated.3.own), channel_id=1, source_target_pairs={{0,3},{1,0},{2,1},{3,2},{4,7},{5,4},{6,5},{7,6},{8,11},{9,8},{10,9... | collective-permute-start | bytes 1572872 | tf_op jit(solution)/shard_map/ppermute | solution.py:613
  77.8 37.4 %collective-permute-start.14 = (bf16[256,2048]{1,0:T(8,128)(2,1)S(1)}, bf16[256,2048]{1,0:T(8,128)(2,1)}, u32[]{:S(2)}, u32[]{:S(2)}) collective-permute-start(bf16[256,2048]{1,0:T(8,128)(2,1)S(1)} %collective-permute-done.13.near_left), channel_id=1, source_target_pairs={{0,4},{4,0},{1,5},{5,1},{2,6},{6,2},{3,7},{7,3},{8,12},{12,8},{9,1... | collective-permute-start | bytes 3145736 | tf_op jit(solution)/shard_map/ppermute | solution.py:681
  78.4 36.7 %collective-permute-start.16 = (bf16[256,2048]{1,0:T(8,128)(2,1)S(1)}, bf16[256,2048]{1,0:T(8,128)(2,1)}, u32[]{:S(2)}, u32[]{:S(2)}) collective-permute-start(bf16[256,2048]{1,0:T(8,128)(2,1)S(1)} %collective-permute-done.15.near_right), channel_id=1, source_target_pairs={{0,4},{4,0},{1,5},{5,1},{2,6},{6,2},{3,7},{7,3},{8,12},{12,8},{9,1... | collective-permute-start | bytes 3145736 | tf_op jit(solution)/shard_map/ppermute | solution.py:681
  78.5 36.6 %collective-permute-start.18 = (bf16[256,2048]{1,0:T(8,128)(2,1)S(1)}, bf16[256,2048]{1,0:T(8,128)(2,1)}, u32[]{:S(2)}, u32[]{:S(2)}) collective-permute-start(bf16[256,2048]{1,0:T(8,128)(2,1)S(1)} %collective-permute-done.17.near_diag), channel_id=1, source_target_pairs={{0,4},{4,0},{1,5},{5,1},{2,6},{6,2},{3,7},{7,3},{8,12},{12,8},{9,1... | collective-permute-start | bytes 3145736 | tf_op jit(solution)/shard_map/ppermute | solution.py:681
  90.0 13.9 %collective-permute-start.9 = (bf16[512,512]{1,0:T(8,128)(2,1)}, bf16[512,512]{1,0:T(8,128)(2,1)S(1)}, u32[]{:S(2)}, u32[]{:S(2)}) collective-permute-start(bf16[512,512]{1,0:T(8,128)(2,1)} %gated.2.own), channel_id=1, source_target_pairs={{0,1},{1,2},{2,3},{3,0},{4,5},{5,6},{6,7},{7,4},{8,9},{9,10},{10,1... | collective-permute-start | bytes 1572872 | tf_op jit(solution)/shard_map/ppermute | solution.py:612
  90.0 13.9 %collective-permute-start.10 = (bf16[512,512]{1,0:T(8,128)(2,1)}, bf16[512,512]{1,0:T(8,128)(2,1)S(1)}, u32[]{:S(2)}, u32[]{:S(2)}) collective-permute-start(bf16[512,512]{1,0:T(8,128)(2,1)} %gated.2.own), channel_id=1, source_target_pairs={{0,3},{1,0},{2,1},{3,2},{4,7},{5,4},{6,5},{7,6},{8,11},{9,8},{10,9... | collective-permute-start | bytes 1572872 | tf_op jit(solution)/shard_map/ppermute | solution.py:613
  111.2 23.3 %collective-permute-start.11 = (bf16[256,512]{1,0:T(8,128)(2,1)}, bf16[256,512]{1,0:T(8,128)(2,1)S(1)}, u32[]{:S(2)}, u32[]{:S(2)}) collective-permute-start(bf16[256,512]{1,0:T(8,128)(2,1)} %slice.16), channel_id=1, source_target_pairs={{0,1},{1,2},{2,3},{3,0},{4,5},{5,6},{6,7},{7,4},{8,9},{9,10},{10,1... | collective-permute-start | bytes 786440 | tf_op jit(solution)/shard_map/ppermute | solution.py:614
  111.3 23.3 %collective-permute-start.12 = (bf16[256,512]{1,0:T(8,128)(2,1)}, bf16[256,512]{1,0:T(8,128)(2,1)}, u32[]{:S(2)}, u32[]{:S(2)}) collective-permute-start(bf16[256,512]{1,0:T(8,128)(2,1)} %slice.17), channel_id=1, source_target_pairs={{0,3},{1,0},{2,1},{3,2},{4,7},{5,4},{6,5},{7,6},{8,11},{9,8},{10,9... | collective-permute-start | bytes 786440 | tf_op jit(solution)/shard_map/ppermute | solution.py:615
  170.8 21.6 %collective-permute-start.27 = (bf16[64,2048]{1,0:T(8,128)(2,1)}, bf16[64,2048]{1,0:T(8,128)(2,1)S(1)}, u32[]{:S(2)}, u32[]{:S(2)}) collective-permute-start(bf16[64,2048]{1,0:T(8,128)(2,1)} %get-tuple-element.53), channel_id=1, source_target_pairs={{0,1},{1,2},{2,3},{3,0},{4,5},{5,6},{6,7},{7,4},{8,9},{9,10},{10,1... | collective-permute-start | bytes 786440 | tf_op jit(solution)/shard_map/ppermute | solution.py:727
  170.8 21.6 %collective-permute-start.28 = (bf16[64,2048]{1,0:T(8,128)(2,1)}, bf16[64,2048]{1,0:T(8,128)(2,1)S(1)}, u32[]{:S(2)}, u32[]{:S(2)}) collective-permute-start(bf16[64,2048]{1,0:T(8,128)(2,1)} %get-tuple-element.55), channel_id=1, source_target_pairs={{0,3},{1,0},{2,1},{3,2},{4,7},{5,4},{6,5},{7,6},{8,11},{9,8},{10,9... | collective-permute-start | bytes 786440 | tf_op jit(solution)/shard_map/ppermute | solution.py:728
  189.7 8.6 %collective-permute-start.19 = (bf16[64,2048]{1,0:T(8,128)(2,1)}, bf16[64,2048]{1,0:T(8,128)(2,1)S(1)}, u32[]{:S(2)}, u32[]{:S(2)}) collective-permute-start(bf16[64,2048]{1,0:T(8,128)(2,1)} %get-tuple-element.44), channel_id=1, source_target_pairs={{0,1},{1,2},{2,3},{3,0},{4,5},{5,6},{6,7},{7,4},{8,9},{9,10},{10,1... | collective-permute-start | bytes 786440 | tf_op jit(solution)/shard_map/ppermute | solution.py:727
  189.7 8.6 %collective-permute-start.20 = (bf16[64,2048]{1,0:T(8,128)(2,1)}, bf16[64,2048]{1,0:T(8,128)(2,1)S(1)}, u32[]{:S(2)}, u32[]{:S(2)}) collective-permute-start(bf16[64,2048]{1,0:T(8,128)(2,1)} %get-tuple-element.46), channel_id=1, source_target_pairs={{0,3},{1,0},{2,1},{3,2},{4,7},{5,4},{6,5},{7,6},{8,11},{9,8},{10,9... | collective-permute-start | bytes 786440 | tf_op jit(solution)/shard_map/ppermute | solution.py:728
  195.6 12.9 %collective-permute-start.29 = (bf16[128,2048]{1,0:T(8,128)(2,1)}, bf16[128,2048]{1,0:T(8,128)(2,1)S(1)}, u32[]{:S(2)}, u32[]{:S(2)}) collective-permute-start(bf16[128,2048]{1,0:T(8,128)(2,1)} %get-tuple-element.56), channel_id=1, source_target_pairs={{0,1},{1,2},{2,3},{3,0},{4,5},{5,6},{6,7},{7,4},{8,9},{9,10},{10,1... | collective-permute-start | bytes 1572872 | tf_op jit(solution)/shard_map/ppermute | solution.py:733
  195.6 12.9 %collective-permute-start.30 = (bf16[128,2048]{1,0:T(8,128)(2,1)}, bf16[128,2048]{1,0:T(8,128)(2,1)S(1)}, u32[]{:S(2)}, u32[]{:S(2)}) collective-permute-start(bf16[128,2048]{1,0:T(8,128)(2,1)} %get-tuple-element.57), channel_id=1, source_target_pairs={{0,3},{1,0},{2,1},{3,2},{4,7},{5,4},{6,5},{7,6},{8,11},{9,8},{10,9... | collective-permute-start | bytes 1572872 | tf_op jit(solution)/shard_map/ppermute | solution.py:734
  201.5 18.2 %collective-permute-start.21 = (bf16[128,2048]{1,0:T(8,128)(2,1)}, bf16[128,2048]{1,0:T(8,128)(2,1)S(1)}, u32[]{:S(2)}, u32[]{:S(2)}) collective-permute-start(bf16[128,2048]{1,0:T(8,128)(2,1)} %get-tuple-element.47), channel_id=1, source_target_pairs={{0,1},{1,2},{2,3},{3,0},{4,5},{5,6},{6,7},{7,4},{8,9},{9,10},{10,1... | collective-permute-start | bytes 1572872 | tf_op jit(solution)/shard_map/ppermute | solution.py:733
  201.5 18.3 %collective-permute-start.22 = (bf16[128,2048]{1,0:T(8,128)(2,1)}, bf16[128,2048]{1,0:T(8,128)(2,1)S(1)}, u32[]{:S(2)}, u32[]{:S(2)}) collective-permute-start(bf16[128,2048]{1,0:T(8,128)(2,1)} %get-tuple-element.48), channel_id=1, source_target_pairs={{0,3},{1,0},{2,1},{3,2},{4,7},{5,4},{6,5},{7,6},{8,11},{9,8},{10,9... | collective-permute-start | bytes 1572872 | tf_op jit(solution)/shard_map/ppermute | solution.py:734
  (38 other events, 280.3 us)
Sparse Core Ops, SparseCore 0:
  9.6 77.5 all-gather.1
